TPU v7x, 32 devices: a whole 2x2x4 slice. The times are simulated.
32 devices in a mesh: sp: 8 (over z, y), tp: 4 (over x, core).
Axes of the slice: x: 2, y: 2, z: 4, core: 2. Of those that a mesh axis runs over, the one named last changes fastest.
Arguments:
- gate_in: bfloat16 [4096, 2048], P('sp', 'tp'), may hold values from -6 to 6
- value_in: bfloat16 [4096, 2048], P('sp', 'tp'), may hold values from -6 to 6
- gate_out: bfloat16 [4096, 2048], P('sp', 'tp'), may hold values from -6 to 6
- conv_taps: float32 [3, 2048], P(None, 'tp'), may hold values from -3.5 to 3.5
- proj_weight: bfloat16 [2048, 2048], P('tp'), may hold values from -0.125 to 0.125
- residual: bfloat16 [4096, 2048], P(('sp', 'tp')), may hold values from -6 to 6
- norm_gain: float32 [2048], replicated, may hold values from 0.1 to 1.9
- routes: int32 [4096, 2], P('sp'), may hold values from 0 to 7, all different within a row; in each aligned block of 128 rows (0 to 127, 128 to 255, ...) at most 64 rows name the same one
- route_weight: float32 [4096, 2], P('sp'), may hold values from 0.1 to 0.9
- expert_gate: bfloat16 [8, 2048, 2048], P('sp', None, 'tp'), may hold values from -0.125 to 0.125
- expert_up: bfloat16 [8, 2048, 2048], P('sp', None, 'tp'), may hold values from -0.125 to 0.125
- expert_down: bfloat16 [8, 2048, 2048], P('sp', 'tp'), may hold values from -0.125 to 0.125
Outputs:
- layer_out: bfloat16 [4096, 2048], P(('sp', 'tp'))
Inputs may be any that keep to these rules, and one draw needn't show every extreme that they name: `routes`: A token's 2 experts differ. In each aligned block of 128 tokens no expert is named by more than 64 tokens, a bound that some block reaches.
All inputs are finite; a program needn't handle non-finite values.
Results may differ from a plain program's by a relative error of at most 0.012.
Values may be sent and summed in bfloat16 or wider, within the bound.
No kernel may reach another device: no remote copies, remote signals or barrier semaphores. Data moves between devices by JAX's collectives and lax.ppermute only.
A program may use at most 128 MiB of HBM per device.

v0:
```python
import jax
import jax.numpy as jnp
from jax import lax
from jax.sharding import PartitionSpec as P


def passed_along(shard, axis, by):
    size = lax.axis_size(axis)
    pairs = [(i, i + by) for i in range(size) if 0 <= i + by < size]
    return lax.ppermute(shard, axis, pairs)


def rounded(values):
    return lax.optimization_barrier(values.astype(jnp.bfloat16)).astype(jnp.float32)


def slot_numbers(route_ids, block_rows, expert_count):
    block_count = route_ids.shape[0] // block_rows
    flat_ids = route_ids.reshape(block_count, block_rows * route_ids.shape[1])
    one_hot = (
        flat_ids[:, :, None] == jnp.arange(expert_count, dtype=jnp.int32)[None, None, :]
    ).astype(jnp.int32)
    before = jnp.cumsum(one_hot, axis=1) - one_hot
    return jnp.sum(before * one_hot, axis=2).reshape(route_ids.shape)


def normalize(hidden_rows, norm_gain):
    inverse = lax.rsqrt(jnp.mean(hidden_rows * hidden_rows, axis=-1, keepdims=True) + 1e-05)
    return (hidden_rows * inverse * norm_gain).astype(jnp.bfloat16)


def dispatch_rows(normed, route_ids, block_rows, expert_count, capacity):
    row_count = route_ids.shape[0]
    top_count = route_ids.shape[1]
    block_count = row_count // block_rows
    slots = slot_numbers(route_ids, block_rows, expert_count)
    row_ids = jnp.arange(row_count, dtype=jnp.int32)
    flat_index = ((row_ids // block_rows)[:, None] * expert_count + route_ids) * capacity + slots
    slot_token = (
        jnp.full((block_count * expert_count * capacity,), row_count, jnp.int32)
        .at[flat_index.reshape(-1)]
        .set(jnp.repeat(row_ids, top_count))
    )
    padded_rows = jnp.concatenate([normed, jnp.zeros((1, normed.shape[1]), jnp.bfloat16)], axis=0)
    outgoing = padded_rows[slot_token].reshape(block_count, expert_count, capacity, normed.shape[1])
    return (outgoing, slots)


def body(
    gate_in,
    value_in,
    gate_out,
    conv_taps,
    proj_weight,
    residual,
    norm_gain,
    routes,
    route_weight,
    expert_gate,
    expert_up,
    expert_down,
):
    tok_dev = gate_in.shape[0]
    model_width = residual.shape[1]
    tp_count = lax.axis_size("tp")
    groups = lax.axis_size("sp")
    quarter = residual.shape[0]
    top_count = routes.shape[1]
    capacity = 2 * quarter * top_count // groups
    tp_index = lax.axis_index("tp")
    first_own = tp_index * quarter
    prior_gate, prior_value = passed_along(
        (gate_in[tok_dev - 2 :], value_in[tok_dev - 2 :]), "sp", 1
    )
    product = gate_in.astype(jnp.float32) * value_in.astype(jnp.float32)
    prior_mix = prior_gate.astype(jnp.float32) * prior_value.astype(jnp.float32)
    padded = jnp.concatenate([prior_mix, product], axis=0)
    conv_sum = conv_taps[0] * padded[:-2] + conv_taps[1] * padded[1:-1] + conv_taps[2] * padded[2:]
    mixed_out = (gate_out.astype(jnp.float32) * conv_sum).astype(jnp.bfloat16)
    own_routes = lax.dynamic_slice_in_dim(routes, first_own, quarter, 0)
    own_weights = lax.dynamic_slice_in_dim(route_weight, first_own, quarter, 0)
    row_block = mixed_out
    summed = lax.psum_scatter(
        rounded(jnp.dot(row_block, proj_weight, preferred_element_type=jnp.float32)).astype(
            jnp.bfloat16
        ),
        "tp",
        scatter_dimension=0,
        tiled=True,
    ).astype(jnp.float32)
    my_rows = residual.astype(jnp.float32) + summed
    normed = normalize(my_rows, norm_gain)
    outgoing, own_slots = dispatch_rows(normed, own_routes, quarter, groups, capacity)
    own_arrived = lax.all_to_all(outgoing, "sp", split_axis=1, concat_axis=1, tiled=True)
    received = lax.all_gather(own_arrived, "tp", axis=0, tiled=True)
    flat_rows = received.reshape(tp_count * groups * capacity, model_width)
    gate_weight = expert_gate[0]
    up_weight = expert_up[0]
    down_weight = expert_down[0]
    row_block = flat_rows
    gate_pre = jnp.dot(row_block, gate_weight, preferred_element_type=jnp.float32)
    up_pre = jnp.dot(row_block, up_weight, preferred_element_type=jnp.float32)
    hidden = (jax.nn.silu(gate_pre) * up_pre).astype(jnp.bfloat16)
    expert_rows = lax.psum_scatter(
        rounded(jnp.dot(hidden, down_weight, preferred_element_type=jnp.float32)).astype(
            jnp.bfloat16
        ),
        "tp",
        scatter_dimension=0,
        tiled=True,
    )
    returned = lax.all_to_all(
        expert_rows.reshape(groups, capacity, model_width),
        "sp",
        split_axis=0,
        concat_axis=0,
        tiled=True,
    )
    flat_pick = own_routes * capacity + own_slots
    picked = returned.reshape(groups * capacity, model_width)[flat_pick]
    weighted = jnp.sum(own_weights[:, :, None] * picked.astype(jnp.float32), axis=1)
    return (my_rows + weighted).astype(jnp.bfloat16)


def solution(mesh):
    placed = (
        P("sp", "tp"),
        P("sp", "tp"),
        P("sp", "tp"),
        P(None, "tp"),
        P("tp", None),
        P(("sp", "tp"), None),
        P(),
        P("sp", None),
        P("sp", None),
        P("sp", None, "tp"),
        P("sp", None, "tp"),
        P("sp", "tp", None),
    )
    return jax.shard_map(
        body, mesh=mesh, in_specs=placed, out_specs=P(("sp", "tp"), None), check_vma=False
    )
```

profile of v0, /device:TPU:0, one launch (start us, length us, event | category | flops | bytes accessed | tf_op | source)
XLA Modules:
  0.0 337.2 jit_solution(5291792366952498572)
XLA Ops:
  6.5 0.9 slice.28
  7.4 5.0 %collective-permute-start = (bf16[2,512]{1,0:T(2,128)(2,1)S(1)}, bf16[2,512]{1,0:T(2,128)(2,1)S(1)}, u32[]{:S(2)}, u32[]{:S(2)}) collective-permute-start(bf16[2,512]{1,0:T(2,128)(2,1)S(1)} %slice.28), channel_id=1, source_target_pairs={{0,4},{4,8},{8,12},{12,16},{16,20},{20,24},{24,28},{1,5},{5,9},{9,... | collective-permute-start | bytes 6152 | tf_op jit(solution)/shard_map/ppermute | solution.py:10
  12.4 0.7 slice.29
  13.1 3.4 %collective-permute-start.1 = (bf16[2,512]{1,0:T(2,128)(2,1)S(1)}, bf16[2,512]{1,0:T(2,128)(2,1)S(1)}, u32[]{:S(2)}, u32[]{:S(2)}) collective-permute-start(bf16[2,512]{1,0:T(2,128)(2,1)S(1)} %slice.29), channel_id=1, source_target_pairs={{0,4},{4,8},{8,12},{12,16},{16,20},{20,24},{24,28},{1,5},{5,9},{9,... | collective-permute-start | bytes 6152 | tf_op jit(solution)/shard_map/ppermute | solution.py:10
  16.6 1.3 convert_multiply_fusion
  18.0 3.8 %convolution_convert_fusion.1 = bf16[512,2048]{1,0:T(8,128)(2,1)} fusion(bf16[512,2048]{1,0:T(8,128)(2,1)S(1)} %copy-done.6, f32[2,512]{1,0:T(2,128)S(1)} %convert_multiply_fusion.1, f32[512,512]{1,0:T(8,128)S(1)} %convert_multiply_fusion, bf16[512,512]{1,0:T(8,128)(2,1)} %param.14, f32[512]{0:T(512)S(1)} %bitcast.44, f32[512]{0:T(512)S(1)} %bitcast.45, ...), kind=kOutput, calls=%fused_computation.5 | convolution fusion | flops 1077411840 | bytes 5777408 | tf_op jit(solution)/shard_map/dot_general | solution.py:84
  21.9 0.7 constant_dynamic-slice_fusion
  22.7 0.1 eq.27
  22.9 0.6 reduce-window.6
  23.5 0.2 slice_reduce_fusion
  23.8 0.1 reshape.195
  24.1 0.1 reshape.196
  24.2 0.1 reshape.222
  24.4 1.4 scatter_custom_fusion
  25.8 29.2 %reduce-scatter.3.cloned.1.call-done = bf16[128,2048]{1,0:T(8,128)(2,1)} async-done(((bf16[512,2048]{1,0:T(8,128)(2,1)}), bf16[128,2048]{1,0:T(8,128)(2,1)}) %reduce-scatter.3.cloned.1.call-update) | async-done | bytes 524304 | tf_op jit(solution)/shard_map/reduce_scatter | solution.py:83
  55.0 1.3 multiply_reduce_fusion.1
  56.3 1.3 multiply_convert_fusion.1
  57.6 3.3 gather_fusion
  61.0 53.7 %all_to_all.10 = bf16[1,8,64,2048]{3,2,0,1:T(8,128)(2,1)} all-to-all(bf16[1,8,64,2048]{3,2,0,1:T(8,128)(2,1)} %bitcast.39), channel_id=1, replica_groups=mesh['sp'=8,'tp'=4] {'sp'}, dimensions={1} | all-to-all | bytes 4194304 | tf_op jit(solution)/shard_map/all_to_all | solution.py:94
  114.8 56.4 %all-gather.2.cloned.1.call-done = bf16[4,8,64,2048]{3,2,1,0:T(8,128)(2,1)} async-done(((bf16[1,8,64,2048]{3,2,1,0:T(8,128)(2,1)}), bf16[4,8,64,2048]{3,2,1,0:T(8,128)(2,1)}) %all-gather.2.cloned.1.call-update) | async-done | bytes 8388624 | tf_op jit(solution)/shard_map/all_gather | solution.py:95
  171.2 7.7 %fusion.2 = f32[2048,512]{1,0:T(8,128)S(1)} fusion(bf16[2048,2048]{1,0:T(8,128)(2,1)} %bitcast.47, bf16[1,2048,512]{2,1,0:T(8,128)(2,1)} %param.21), kind=kOutput, calls=%fused_computation.8 | convolution fusion | flops 4294967296 | bytes 14680064 | tf_op jit(solution)/shard_map/dot_general | solution.py:101
  178.9 5.2 %multiply_convert_fusion = bf16[2048,512]{1,0:T(8,128)(2,1)S(1)} fusion(f32[2048,512]{1,0:T(8,128)S(1)} %fusion.2, bf16[2048,2048]{1,0:T(8,128)(2,1)S(1)} %bitcast.48, bf16[1,2048,512]{2,1,0:T(8,128)(2,1)S(1)} %copy-done.7), kind=kOutput, calls=%fused_computation.4 | convolution fusion | flops 4301258752 | bytes 16777216 | tf_op jit(solution)/shard_map/dot_general | solution.py:102
  184.1 6.8 %convolution_convert_fusion = bf16[2048,2048]{1,0:T(8,128)(2,1)} fusion(bf16[2048,512]{1,0:T(8,128)(2,1)S(1)} %multiply_convert_fusion, bf16[1,512,2048]{2,1,0:T(8,128)(2,1)S(1)} %copy-done), kind=kOutput, calls=%fused_computation.3 | convolution fusion | flops 4299161600 | bytes 12582912 | tf_op jit(solution)/shard_map/dot_general | solution.py:105
  190.9 71.5 %reduce-scatter.5.cloned.1.call-done = bf16[512,2048]{1,0:T(8,128)(2,1)} async-done(((bf16[2048,2048]{1,0:T(8,128)(2,1)}), bf16[512,2048]{1,0:T(8,128)(2,1)}) %reduce-scatter.5.cloned.1.call-update) | async-done | bytes 2097168 | tf_op jit(solution)/shard_map/reduce_scatter | solution.py:104
  262.5 5.5 %all-to-all-start.1 = ((bf16[8,64,2048]{2,1,0:T(8,128)(2,1)}), bf16[8,64,2048]{2,1,0:T(8,128)(2,1)}, u32[]{:S(2)}, u32[]{:S(2)}) async-start(bf16[8,64,2048]{2,1,0:T(8,128)(2,1)} %bitcast.41), calls=%async_computation.3 | async-start | bytes 4194304 | tf_op jit(solution)/shard_map/all_to_all | solution.py:112
  268.0 0.1 reshape.212
  268.1 0.7 constant_dynamic-slice_fusion.1
  268.9 47.2 %all-to-all-done.1 = bf16[8,64,2048]{2,1,0:T(8,128)(2,1)} async-done(((bf16[8,64,2048]{2,1,0:T(8,128)(2,1)}), bf16[8,64,2048]{2,1,0:T(8,128)(2,1)}, u32[]{:S(2)}, u32[]{:S(2)}) %all-to-all-start.1) | async-done | bytes 2097184 | tf_op jit(solution)/shard_map/all_to_all | solution.py:112
  316.2 5.2 %gather_fusion.1 = bf16[256,2048]{1,0:T(8,128)(2,1)} fusion(bf16[512,2048]{1,0:T(8,128)(2,1)} %bitcast.18, s32[1024]{0:T(1024)S(1)} %pad_clamp_fusion), kind=kCustom, calls=%fused_computation.1 | custom fusion | bytes 2098176 | tf_op jit(solution)/shard_map/gather | solution.py:120
  321.4 3.4 %reshape.229 = f32[128,2,2048]{2,1,0:T(2,128)} reshape(bf16[256,2048]{1,0:T(8,128)(2,1)} %gather_fusion.1) | data formatting | bytes 3145728 | tf_op jit(solution)/shard_map/convert_element_type | solution.py:121
  324.8 4.9 %multiply_reduce_fusion = f32[128,2048]{1,0:T(8,128)S(1)} fusion(f32[128,2,2048]{2,1,0:T(2,128)} %reshape.229, f32[128,2]{1,0:T(8,128)S(1)} %copy.16), kind=kLoop, calls=%fused_computation.10 | loop fusion | flops 786432 | bytes 3146752 | tf_op jit(solution)/shard_map/reduce_sum | solution.py:121
  329.7 1.0 add_convert_fusion
  (41 shorter events, 0.7 us)
Async XLA Ops:
  6.5 177.6 %copy-start = (bf16[1,512,2048]{2,1,0:T(8,128)(2,1)S(1)}, bf16[1,512,2048]{2,1,0:T(8,128)(2,1)}, u32[]{:S(2)}) copy-start(bf16[1,512,2048]{2,1,0:T(8,128)(2,1)} %param.23) | copy-start | bytes 6291460
  6.5 11.4 %copy-start.4 = (f32[3,512]{1,0:T(4,128)S(1)}, f32[3,512]{1,0:T(4,128)}, u32[]{:S(2)}) copy-start(f32[3,512]{1,0:T(4,128)} %param.15) | copy-start | bytes 18436
  6.5 48.5 %reduce-scatter.3.cloned.1.call-start = ((), (), s32[]{:S(2)}) async-start(), calls=%async_computation.4 | async-start | bytes 2621440 | tf_op jit(solution)/shard_map/reduce_scatter | solution.py:83
  6.5 11.4 %copy-start.6 = (bf16[512,2048]{1,0:T(8,128)(2,1)S(1)}, bf16[512,2048]{1,0:T(8,128)(2,1)}, u32[]{:S(2)}) copy-start(bf16[512,2048]{1,0:T(8,128)(2,1)} %param.16) | copy-start | bytes 6291460
  7.4 10.5 %collective-permute-start = (bf16[2,512]{1,0:T(2,128)(2,1)S(1)}, bf16[2,512]{1,0:T(2,128)(2,1)S(1)}, u32[]{:S(2)}, u32[]{:S(2)}) collective-permute-start(bf16[2,512]{1,0:T(2,128)(2,1)S(1)} %slice.28), channel_id=1, source_target_pairs={{0,4},{4,8},{8,12},{12,16},{16,20},{20,24},{24,28},{1,5},{5,9},{9,... | collective-permute-start | bytes 6152 | tf_op jit(solution)/shard_map/ppermute | solution.py:10
  13.1 4.8 %collective-permute-start.1 = (bf16[2,512]{1,0:T(2,128)(2,1)S(1)}, bf16[2,512]{1,0:T(2,128)(2,1)S(1)}, u32[]{:S(2)}, u32[]{:S(2)}) collective-permute-start(bf16[2,512]{1,0:T(2,128)(2,1)S(1)} %slice.29), channel_id=1, source_target_pairs={{0,4},{4,8},{8,12},{12,16},{16,20},{20,24},{24,28},{1,5},{5,9},{9,... | collective-permute-start | bytes 6152 | tf_op jit(solution)/shard_map/ppermute | solution.py:10
  21.8 33.2 %copy-start.1 = (bf16[128,2048]{1,0:T(8,128)(2,1)S(1)}, bf16[128,2048]{1,0:T(8,128)(2,1)}, u32[]{:S(2)}) copy-start(bf16[128,2048]{1,0:T(8,128)(2,1)} %param.17) | copy-start | bytes 1572868
  21.8 34.5 %copy-start.3 = (f32[2048]{0:T(1024)S(1)}, f32[2048]{0:T(1024)}, u32[]{:S(2)}) copy-start(f32[2048]{0:T(1024)} %param.18) | copy-start | bytes 24580
  21.8 149.4 %all-gather.2.cloned.1.call-start = ((), (), s32[]{:S(2)}) async-start(), calls=%async_computation.5 | async-start | bytes 10485760 | tf_op jit(solution)/shard_map/all_gather | solution.py:95
  114.7 147.8 %reduce-scatter.5.cloned.1.call-start = ((), (), s32[]{:S(2)}) async-start(), calls=%async_computation.6 | async-start | bytes 10485760 | tf_op jit(solution)/shard_map/reduce_scatter | solution.py:104
  171.2 7.7 %copy-start.5 = (bf16[4,8,64,2048]{3,2,1,0:T(8,128)(2,1)S(1)}, bf16[4,8,64,2048]{3,2,1,0:T(8,128)(2,1)}, u32[]{:S(2)}) copy-start(bf16[4,8,64,2048]{3,2,1,0:T(8,128)(2,1)} %all-gather.2.cloned.1.call-done) | copy-start | bytes 25165828
  171.2 7.7 %copy-start.7 = (bf16[1,2048,512]{2,1,0:T(8,128)(2,1)S(1)}, bf16[1,2048,512]{2,1,0:T(8,128)(2,1)}, u32[]{:S(2)}) copy-start(bf16[1,2048,512]{2,1,0:T(8,128)(2,1)} %param.22) | copy-start | bytes 6291460
  262.5 53.7 %all-to-all-start.1 = ((bf16[8,64,2048]{2,1,0:T(8,128)(2,1)}), bf16[8,64,2048]{2,1,0:T(8,128)(2,1)}, u32[]{:S(2)}, u32[]{:S(2)}) async-start(bf16[8,64,2048]{2,1,0:T(8,128)(2,1)} %bitcast.41), calls=%async_computation.3 | async-start | bytes 4194304 | tf_op jit(solution)/shard_map/all_to_all | solution.py:112
  324.8 4.9 %copy-start.2 = (bf16[128,2048]{1,0:T(8,128)(2,1)S(1)}, bf16[128,2048]{1,0:T(8,128)(2,1)}, u32[]{:S(2)}) copy-start(bf16[128,2048]{1,0:T(8,128)(2,1)} %reduce-scatter.3.cloned.1.call-done) | copy-start | bytes 1572868
Sparse Core Ops, SparseCore 0:
  22.0 32.9 reduce-scatter.2
  114.8 56.3 all-gather.1
  191.0 71.3 reduce-scatter.4
where the time goes:
time: 338 us; the launch traced here: 337 us
  waiting for transfers between devices  204 us (60%)
  blocking collectives  53.7 us (16%)
  matrix products  23.5 us (7%)
  local copies, waits for them, and re-layouts  17.5 us (5%)
  starting transfers between devices  14 us (4%)
  between operations  13.4 us (4%)
  other arithmetic  10.6 us (3%)
    reduce_scatter x1, waiting for transfers between devices, body(): lax.psum_scatter(rounded(jnp.dot(hidden, down_weight, preferred_element_t...  71.5 us
    all_gather x1, waiting for transfers between devices, body(): received = lax.all_gather(own_arrived, 'tp', axis=0, tiled=True)  56.4 us
    all_to_all x1, blocking collectives, body(): lax.all_to_all(outgoing, 'sp', split_axis=1, concat_axis=1, tiled=True)  53.7 us
    all_to_all x1, waiting for transfers between devices, body(): lax.all_to_all(expert_rows.reshape(groups, capacity, model_width), 'sp',...  47.2 us
    reduce_scatter x1, waiting for transfers between devices, body(): lax.psum_scatter(rounded(jnp.dot(row_block, proj_weight, preferred_elemen...  29.2 us
    ppermute x2, starting transfers between devices, passed_along(): return lax.ppermute(shard, axis, pairs)  8.43 us
    dot_general x1, matrix products, body(): jnp.dot(row_block, gate_weight, preferred_element_type=jnp.float32)  7.67 us
    dot_general x1, matrix products, body(): jnp.dot(hidden, down_weight, preferred_element_type=jnp.float32)  6.79 us
  transfers between devices with their start and end apart: 6, of which 4 were waited for; matrix products, arithmetic and copies ran while one was open for 2% of the time, Pallas kernels for 0%

commit v1 on v0

v1 whole, which is shorter than its diff:
```python
import jax
import jax.numpy as jnp
from jax import lax
from jax.sharding import PartitionSpec as P


def swapped(values, axis, distance):
    size = lax.axis_size(axis)
    return lax.ppermute(values, axis, [(i, i ^ distance) for i in range(size)])


def passed_along(shard, axis, by):
    size = lax.axis_size(axis)
    pairs = [(i, i + by) for i in range(size) if 0 <= i + by < size]
    return lax.ppermute(shard, axis, pairs)


def product_of(left, right):
    return jnp.dot(left, right, preferred_element_type=jnp.float32)


def narrow(values):
    return values.astype(jnp.bfloat16)


def wide(values):
    return values.astype(jnp.float32)


def normalize(hidden_rows, norm_gain):
    inverse = lax.rsqrt(jnp.mean(hidden_rows * hidden_rows, axis=-1, keepdims=True) + 1e-05)
    return (hidden_rows * inverse * norm_gain).astype(jnp.bfloat16)


def body(
    gate_in,
    value_in,
    gate_out,
    conv_taps,
    proj_weight,
    residual,
    norm_gain,
    routes,
    route_weight,
    expert_gate,
    expert_up,
    expert_down,
):
    tok_dev = gate_in.shape[0]
    model_width = residual.shape[1]
    groups = lax.axis_size("sp")
    quarter = residual.shape[0]
    top_count = routes.shape[1]
    capacity = 2 * quarter * top_count // groups
    tp_index = lax.axis_index("tp")
    sp_index = lax.axis_index("sp")
    pairwise = groups <= 8

    halo = passed_along(
        jnp.concatenate([gate_in[tok_dev - 2 :], value_in[tok_dev - 2 :]], axis=0), "sp", 1
    )
    product = wide(gate_in) * wide(value_in)
    padded = jnp.concatenate([wide(halo[:2]) * wide(halo[2:]), product], axis=0)
    conv_sum = conv_taps[0] * padded[:-2] + conv_taps[1] * padded[1:-1] + conv_taps[2] * padded[2:]
    mixed_out = narrow(wide(gate_out) * conv_sum)

    def rows_for(distance):
        return lax.dynamic_slice_in_dim(mixed_out, (tp_index ^ distance) * quarter, quarter, 0)

    far = narrow(product_of(jnp.concatenate([rows_for(3), rows_for(2)], axis=0), proj_weight))
    far_other = swapped(far[:quarter], "tp", 1)
    far_sum = swapped(narrow(wide(far[quarter:]) + wide(far_other)), "tp", 2)
    near = narrow(product_of(jnp.concatenate([rows_for(1), rows_for(0)], axis=0), proj_weight))
    near_other = swapped(near[:quarter], "tp", 1)
    my_rows = wide(residual) + (wide(near[quarter:]) + wide(near_other) + wide(far_sum))
    normed = normalize(my_rows, norm_gain)

    own_routes = lax.dynamic_slice_in_dim(routes, tp_index * quarter, quarter, 0)
    own_weights = lax.dynamic_slice_in_dim(route_weight, tp_index * quarter, quarter, 0)
    experts = jnp.arange(groups, dtype=jnp.int32)
    if pairwise:
        experts = experts ^ sp_index
    named = own_routes.T[:, None, :] == experts[None, :, None]
    any_named = jnp.any(named, axis=0)
    token = jnp.arange(quarter, dtype=jnp.int32)
    earlier = (token[:, None] < token[None, :]).astype(jnp.bfloat16)
    slots = product_of(any_named.astype(jnp.bfloat16), earlier).astype(jnp.int32)
    slot = jnp.arange(capacity, dtype=jnp.int32)
    at_slot = slots[:, None, :] == slot[None, :, None]
    select = (any_named[:, None, :] & at_slot).astype(jnp.bfloat16)
    place = (named[:, :, None, :] & at_slot[None]).astype(jnp.bfloat16)

    gate_weight = expert_gate[0]
    up_weight = expert_up[0]
    down_weight = expert_down[0]

    def expert(rows):
        gate_pre = product_of(rows, gate_weight)
        up_pre = product_of(rows, up_weight)
        hidden = lax.optimization_barrier(narrow(jax.nn.silu(gate_pre) * up_pre))
        return narrow(product_of(hidden, down_weight))

    def gathered(own):
        across = swapped(own, "tp", 2)
        return (swapped(across, "tp", 1), across, swapped(own, "tp", 1), own)

    def scattered(rows, count):
        far_other = swapped(rows[:count], "tp", 1)
        far_part = narrow(wide(rows[count : 2 * count]) + wide(far_other))
        far_sum = swapped(far_part, "tp", 2)
        near_other = swapped(rows[2 * count : 3 * count], "tp", 1)
        return narrow(wide(rows[3 * count :]) + wide(near_other) + wide(far_sum))

    def send(pieces, first):
        if not pairwise:
            return lax.all_to_all(pieces, "sp", split_axis=0, concat_axis=0, tiled=True)
        moved = []
        for m in range(pieces.shape[0]):
            piece = pieces[m : m + 1]
            if first + m > 0:
                piece = swapped(piece, "sp", first + m)
            moved.append(piece)
        return jnp.concatenate(moved, axis=0)

    size = max(1, groups // 4) if pairwise else groups
    starts = list(range(0, groups, size))
    order = starts[:2] + starts[:1:-1]
    arrived = {}
    for first in order:
        chosen = select[first : first + size].reshape(size * capacity, quarter)
        outgoing = narrow(product_of(chosen, normed))
        arrived[first] = send(outgoing.reshape(size, capacity, model_width), first)
    results = {}
    for first in order:
        own = arrived[first].reshape(size * capacity, model_width)
        blocks = gathered(own)
        rows = expert(jnp.concatenate(blocks, axis=0))
        results[first] = scattered(rows, size * capacity)
    total = my_rows
    for first in order:
        returned = send(results[first].reshape(size, capacity, model_width), first)
        returned = returned.reshape(size * capacity, model_width)
        for k in range(top_count):
            chosen = place[k, first : first + size].reshape(size * capacity, quarter)
            picked = lax.dot_general(
                chosen, returned, (((0,), (0,)), ((), ())), preferred_element_type=jnp.float32
            )
            total = total + own_weights[:, k : k + 1] * picked
    return narrow(total)


def solution(mesh):
    placed = (
        P("sp", "tp"),
        P("sp", "tp"),
        P("sp", "tp"),
        P(None, "tp"),
        P("tp", None),
        P(("sp", "tp"), None),
        P(),
        P("sp", None),
        P("sp", None),
        P("sp", None, "tp"),
        P("sp", None, "tp"),
        P("sp", "tp", None),
    )

    return jax.shard_map(
        body, mesh=mesh, in_specs=placed, out_specs=P(("sp", "tp"), None), check_vma=False
    )
```

time: 338 us -> 209 us (0.62)
  waiting for transfers between devices: 204 us -> 130 us
  blocking collectives: 53.7 us -> 0 us
  starting transfers between devices: 14 us -> 46.2 us
  local copies, waits for them, and re-layouts: 17.5 us -> 3.91 us
  between operations: 13.4 us -> 0.78 us
  other arithmetic: 10.6 us -> 6.04 us
    ppermute x0 -> x41, waiting for transfers between devices: none -> 130 us  [swapped(): return lax.ppermute(values, axis, [(i, i ^ distance) for i in range(size)])]
    reduce_scatter x2 -> x0, waiting for transfers between devices: 101 us -> none  [the longest x1 71.5 us: body(): lax.psum_scatter(rounded(jnp.dot(hidden, down_weight, preferred_element_t...]
    all_gather x1 -> x0, waiting for transfers between devices: 56.4 us -> none  [body(): received = lax.all_gather(own_arrived, 'tp', axis=0, tiled=True)]
    all_to_all x1 -> x0, blocking collectives: 53.7 us -> none  [body(): lax.all_to_all(outgoing, 'sp', split_axis=1, concat_axis=1, tiled=True)]
    all_to_all x1 -> x0, waiting for transfers between devices: 47.2 us -> none  [body(): lax.all_to_all(expert_rows.reshape(groups, capacity, model_width), 'sp',...]
    ppermute x0 -> x41, starting transfers between devices: none -> 41.3 us  [swapped(): return lax.ppermute(values, axis, [(i, i ^ distance) for i in range(size)])]
    gather x2 -> x0, local copies, waits for them, and re-layouts: 8.55 us -> none  [the longest x1 5.21 us: body(): picked = returned.reshape(groups * capacity, model_width)[flat_pick]]
    all_to_all x1 -> x0, starting transfers between devices: 5.52 us -> none  [body(): lax.all_to_all(expert_rows.reshape(groups, capacity, model_width), 'sp',...]
  transfers between devices with their start and end apart: 6 -> 42, of which waited for: 4 -> 18; matrix products, arithmetic and copies ran while one was open for 2% -> 12% of each run, Pallas kernels for 0% -> 0%
where the time goes in v1:
time: 209 us
  waiting for transfers between devices  130 us (62%)
  starting transfers between devices  46.2 us (22%)
  matrix products  22.1 us (11%)
  other arithmetic  6.04 us (3%)
  local copies, waits for them, and re-layouts  3.91 us (2%)
    ppermute x41, waiting for transfers between devices, swapped(): return lax.ppermute(values, axis, [(i, i ^ distance) for i in range(size)])  130 us
    ppermute x41, starting transfers between devices, swapped(): return lax.ppermute(values, axis, [(i, i ^ distance) for i in range(size)])  41.3 us
    dot_general x19, matrix products, product_of(): return jnp.dot(left, right, preferred_element_type=jnp.float32)  18.3 us
    ppermute x1, starting transfers between devices, passed_along(): return lax.ppermute(shard, axis, pairs)  4.9 us
  transfers between devices with their start and end apart: 42, of which 18 were waited for; matrix products, arithmetic and copies ran while one was open for 12% of the time, Pallas kernels for 0%

profile of v1, /device:TPU:0, one launch (start us, length us, event | category | flops | bytes accessed | tf_op | source)
XLA Modules:
  0.0 209.2 jit_solution(3106955984216906990)
XLA Ops:
  1.6 4.9 %collective-permute-start = (bf16[4,512]{1,0:T(4,128)(2,1)S(1)}, bf16[4,512]{1,0:T(4,128)(2,1)S(1)}, u32[]{:S(2)}, u32[]{:S(2)}) collective-permute-start(bf16[4,512]{1,0:T(4,128)(2,1)S(1)} %pad_maximum_fusion.29), channel_id=1, source_target_pairs={{0,4},{4,8},{8,12},{12,16},{16,20},{20,24},{24,28},{1,5},{5,9},{9,... | collective-permute-start | bytes 12296 | tf_op jit(solution)/shard_map/ppermute | solution.py:15
  8.9 1.6 fusion.34
  13.5 1.6 collective-permute-start.3
  15.9 11.7 %collective-permute-done.3 = bf16[128,2048]{1,0:T(8,128)(2,1)S(1)} collective-permute-done((bf16[128,2048]{1,0:T(8,128)(2,1)S(1)}, bf16[128,2048]{1,0:T(8,128)(2,1)S(1)}, u32[]{:S(2)}, u32[]{:S(2)}) %collective-permute-start.3) | collective-permute-done | bytes 524320 | tf_op jit(solution)/shard_map/ppermute | solution.py:9
  28.8 2.6 %collective-permute-start.13 = (bf16[1,64,2048]{2,1,0:T(8,128)(2,1)S(1)}, bf16[1,64,2048]{2,1,0:T(8,128)(2,1)S(1)}, u32[]{:S(2)}, u32[]{:S(2)}) collective-permute-start(bf16[1,64,2048]{2,1,0:T(8,128)(2,1)S(1)} %get-tuple-element.28), channel_id=1, source_target_pairs={{0,12},{4,8},{8,4},{12,0},{16,28},{20,24},{24,20},{28,16},{1,13},{... | collective-permute-start | bytes 786440 | tf_op jit(solution)/shard_map/ppermute | solution.py:9
  33.1 4.1 %collective-permute-start.23 = (bf16[1,64,2048]{2,1,0:T(8,128)(2,1)S(1)}, bf16[1,64,2048]{2,1,0:T(8,128)(2,1)S(1)}, u32[]{:S(2)}, u32[]{:S(2)}) collective-permute-start(bf16[1,64,2048]{2,1,0:T(8,128)(2,1)S(1)} %get-tuple-element.20), channel_id=1, source_target_pairs={{0,28},{4,24},{8,20},{12,16},{16,12},{20,8},{24,4},{28,0},{1,29},{... | collective-permute-start | bytes 786440 | tf_op jit(solution)/shard_map/ppermute | solution.py:9
  39.0 4.8 %collective-permute-done.12 = bf16[1,64,2048]{2,1,0:T(8,128)(2,1)S(1)} collective-permute-done((bf16[1,64,2048]{2,1,0:T(8,128)(2,1)S(1)}, bf16[1,64,2048]{2,1,0:T(8,128)(2,1)S(1)}, u32[]{:S(2)}, u32[]{:S(2)}) %collective-permute-start.12) | collective-permute-done | bytes 262176 | tf_op jit(solution)/shard_map/ppermute | solution.py:9
  43.8 1.6 collective-permute-start.14
  45.4 3.9 %collective-permute-start.33 = (bf16[1,64,2048]{2,1,0:T(8,128)(2,1)S(1)}, bf16[1,64,2048]{2,1,0:T(8,128)(2,1)S(1)}, u32[]{:S(2)}, u32[]{:S(2)}) collective-permute-start(bf16[1,64,2048]{2,1,0:T(8,128)(2,1)S(1)} %get-tuple-element.16), channel_id=1, source_target_pairs={{0,20},{4,16},{8,28},{12,24},{16,4},{20,0},{24,12},{28,8},{1,21},{... | collective-permute-start | bytes 786440 | tf_op jit(solution)/shard_map/ppermute | solution.py:9
  50.6 2.1 %collective-permute-done.23 = bf16[1,64,2048]{2,1,0:T(8,128)(2,1)S(1)} collective-permute-done((bf16[1,64,2048]{2,1,0:T(8,128)(2,1)S(1)}, bf16[1,64,2048]{2,1,0:T(8,128)(2,1)S(1)}, u32[]{:S(2)}, u32[]{:S(2)}) %collective-permute-start.23) | collective-permute-done | bytes 262176 | tf_op jit(solution)/shard_map/ppermute | solution.py:9
  52.8 5.3 %collective-permute-done.22 = bf16[1,64,2048]{2,1,0:T(8,128)(2,1)S(1)} collective-permute-done((bf16[1,64,2048]{2,1,0:T(8,128)(2,1)S(1)}, bf16[1,64,2048]{2,1,0:T(8,128)(2,1)S(1)}, u32[]{:S(2)}, u32[]{:S(2)}) %collective-permute-start.22) | collective-permute-done | bytes 262176 | tf_op jit(solution)/shard_map/ppermute | solution.py:9
  58.0 1.5 collective-permute-start.5
  59.6 20.3 %collective-permute-done.33 = bf16[1,64,2048]{2,1,0:T(8,128)(2,1)S(1)} collective-permute-done((bf16[1,64,2048]{2,1,0:T(8,128)(2,1)S(1)}, bf16[1,64,2048]{2,1,0:T(8,128)(2,1)S(1)}, u32[]{:S(2)}, u32[]{:S(2)}) %collective-permute-start.33) | collective-permute-done | bytes 262176 | tf_op jit(solution)/shard_map/ppermute | solution.py:9
  79.9 3.4 %collective-permute-done.32 = bf16[1,64,2048]{2,1,0:T(8,128)(2,1)S(1)} collective-permute-done((bf16[1,64,2048]{2,1,0:T(8,128)(2,1)S(1)}, bf16[1,64,2048]{2,1,0:T(8,128)(2,1)S(1)}, u32[]{:S(2)}, u32[]{:S(2)}) %collective-permute-start.32) | collective-permute-done | bytes 262176 | tf_op jit(solution)/shard_map/ppermute | solution.py:9
  83.4 1.6 collective-permute-start.24
  90.1 8.2 %collective-permute-done.24 = bf16[128,2048]{1,0:T(8,128)(2,1)S(1)} collective-permute-done((bf16[128,2048]{1,0:T(8,128)(2,1)S(1)}, bf16[128,2048]{1,0:T(8,128)(2,1)S(1)}, u32[]{:S(2)}, u32[]{:S(2)}) %collective-permute-start.24) | collective-permute-done | bytes 524320 | tf_op jit(solution)/shard_map/ppermute | solution.py:9
  98.3 10.8 %collective-permute-done.34 = bf16[128,2048]{1,0:T(8,128)(2,1)S(1)} collective-permute-done((bf16[128,2048]{1,0:T(8,128)(2,1)S(1)}, bf16[128,2048]{1,0:T(8,128)(2,1)S(1)}, u32[]{:S(2)}, u32[]{:S(2)}) %collective-permute-start.34) | collective-permute-done | bytes 524320 | tf_op jit(solution)/shard_map/ppermute | solution.py:9
  114.1 1.4 fusion.23
  123.7 1.5 collective-permute-start.19
  125.8 1.5 collective-permute-start.10
  127.3 11.2 %collective-permute-done.19 = bf16[128,2048]{1,0:T(8,128)(2,1)S(1)} collective-permute-done((bf16[128,2048]{1,0:T(8,128)(2,1)S(1)}, bf16[128,2048]{1,0:T(8,128)(2,1)S(1)}, u32[]{:S(2)}, u32[]{:S(2)}) %collective-permute-start.19) | collective-permute-done | bytes 524320 | tf_op jit(solution)/shard_map/ppermute | solution.py:9
  138.6 1.5 collective-permute-start.29
  141.0 8.8 %collective-permute-done.10 = bf16[128,2048]{1,0:T(8,128)(2,1)S(1)} collective-permute-done((bf16[128,2048]{1,0:T(8,128)(2,1)S(1)}, bf16[128,2048]{1,0:T(8,128)(2,1)S(1)}, u32[]{:S(2)}, u32[]{:S(2)}) %collective-permute-start.10) | collective-permute-done | bytes 524320 | tf_op jit(solution)/shard_map/ppermute | solution.py:9
  150.1 2.4 %collective-permute-start.20 = (bf16[1,64,2048]{2,1,0:T(8,128)(2,1)S(1)}, bf16[1,64,2048]{2,1,0:T(8,128)(2,1)S(1)}, u32[]{:S(2)}, u32[]{:S(2)}) collective-permute-start(bf16[1,64,2048]{2,1,0:T(8,128)(2,1)S(1)} %get-tuple-element.25), channel_id=1, source_target_pairs={{0,8},{4,12},{8,0},{12,4},{16,24},{20,28},{24,16},{28,20},{1,9},{5... | collective-permute-start | bytes 786440 | tf_op jit(solution)/shard_map/ppermute | solution.py:9
  152.5 8.5 %collective-permute-done.29 = bf16[128,2048]{1,0:T(8,128)(2,1)S(1)} collective-permute-done((bf16[128,2048]{1,0:T(8,128)(2,1)S(1)}, bf16[128,2048]{1,0:T(8,128)(2,1)S(1)}, u32[]{:S(2)}, u32[]{:S(2)}) %collective-permute-start.29) | collective-permute-done | bytes 524320 | tf_op jit(solution)/shard_map/ppermute | solution.py:9
  162.2 3.1 %collective-permute-start.31 = (bf16[1,64,2048]{2,1,0:T(8,128)(2,1)S(1)}, bf16[1,64,2048]{2,1,0:T(8,128)(2,1)S(1)}, u32[]{:S(2)}, u32[]{:S(2)}) collective-permute-start(bf16[1,64,2048]{2,1,0:T(8,128)(2,1)S(1)} %get-tuple-element.18), channel_id=1, source_target_pairs={{0,28},{4,24},{8,20},{12,16},{16,12},{20,8},{24,4},{28,0},{1,29},{... | collective-permute-start | bytes 786440 | tf_op jit(solution)/shard_map/ppermute | solution.py:9
  165.3 6.0 %collective-permute-done.39 = bf16[128,2048]{1,0:T(8,128)(2,1)S(1)} collective-permute-done((bf16[128,2048]{1,0:T(8,128)(2,1)S(1)}, bf16[128,2048]{1,0:T(8,128)(2,1)S(1)}, u32[]{:S(2)}, u32[]{:S(2)}) %collective-permute-start.39) | collective-permute-done | bytes 524320 | tf_op jit(solution)/shard_map/ppermute | solution.py:9
  171.4 2.5 %collective-permute-start.30 = (bf16[1,64,2048]{2,1,0:T(8,128)(2,1)S(1)}, bf16[1,64,2048]{2,1,0:T(8,128)(2,1)S(1)}, u32[]{:S(2)}, u32[]{:S(2)}) collective-permute-start(bf16[1,64,2048]{2,1,0:T(8,128)(2,1)S(1)} %get-tuple-element.17), channel_id=1, source_target_pairs={{0,24},{4,28},{8,16},{12,20},{16,8},{20,12},{24,0},{28,4},{1,25},{... | collective-permute-start | bytes 786440 | tf_op jit(solution)/shard_map/ppermute | solution.py:9
  174.3 3.3 %collective-permute-start.40 = (bf16[1,64,2048]{2,1,0:T(8,128)(2,1)S(1)}, bf16[1,64,2048]{2,1,0:T(8,128)(2,1)S(1)}, u32[]{:S(2)}, u32[]{:S(2)}) collective-permute-start(bf16[1,64,2048]{2,1,0:T(8,128)(2,1)S(1)} %get-tuple-element.13), channel_id=1, source_target_pairs={{0,16},{4,20},{8,24},{12,28},{16,0},{20,4},{24,8},{28,12},{1,17},{... | collective-permute-start | bytes 786440 | tf_op jit(solution)/shard_map/ppermute | solution.py:9
  179.3 3.1 %collective-permute-done.30 = bf16[1,64,2048]{2,1,0:T(8,128)(2,1)S(1)} collective-permute-done((bf16[1,64,2048]{2,1,0:T(8,128)(2,1)S(1)}, bf16[1,64,2048]{2,1,0:T(8,128)(2,1)S(1)}, u32[]{:S(2)}, u32[]{:S(2)}) %collective-permute-start.30) | collective-permute-done | bytes 262176 | tf_op jit(solution)/shard_map/ppermute | solution.py:9
  183.2 20.7 %collective-permute-done.41 = bf16[1,64,2048]{2,1,0:T(8,128)(2,1)S(1)} collective-permute-done((bf16[1,64,2048]{2,1,0:T(8,128)(2,1)S(1)}, bf16[1,64,2048]{2,1,0:T(8,128)(2,1)S(1)}, u32[]{:S(2)}, u32[]{:S(2)}) %collective-permute-start.41) | collective-permute-done | bytes 262176 | tf_op jit(solution)/shard_map/ppermute | solution.py:9
  203.9 3.7 %collective-permute-done.40 = bf16[1,64,2048]{2,1,0:T(8,128)(2,1)S(1)} collective-permute-done((bf16[1,64,2048]{2,1,0:T(8,128)(2,1)S(1)}, bf16[1,64,2048]{2,1,0:T(8,128)(2,1)S(1)}, u32[]{:S(2)}, u32[]{:S(2)}) %collective-permute-start.40) | collective-permute-done | bytes 262176 | tf_op jit(solution)/shard_map/ppermute | solution.py:9
  (144 shorter events, 39.2 us)
Async XLA Ops:
  13.5 14.0 %collective-permute-start.3 = (bf16[128,2048]{1,0:T(8,128)(2,1)S(1)}, bf16[128,2048]{1,0:T(8,128)(2,1)S(1)}, u32[]{:S(2)}, u32[]{:S(2)}) collective-permute-start(bf16[128,2048]{1,0:T(8,128)(2,1)S(1)} %add_convert_fusion.8), channel_id=1, source_target_pairs={{0,2},{1,3},{2,0},{3,1},{4,6},{5,7},{6,4},{7,5},{8,10},{9,11},{10,... | collective-permute-start | bytes 1572872 | tf_op jit(solution)/shard_map/ppermute | solution.py:9
  31.4 12.4 %collective-permute-start.12 = (bf16[1,64,2048]{2,1,0:T(8,128)(2,1)S(1)}, bf16[1,64,2048]{2,1,0:T(8,128)(2,1)S(1)}, u32[]{:S(2)}, u32[]{:S(2)}) collective-permute-start(bf16[1,64,2048]{2,1,0:T(8,128)(2,1)S(1)} %get-tuple-element.27), channel_id=1, source_target_pairs={{0,8},{4,12},{8,0},{12,4},{16,24},{20,28},{24,16},{28,20},{1,9},{5... | collective-permute-start | bytes 786440 | tf_op jit(solution)/shard_map/ppermute | solution.py:9
  32.2 17.1 %collective-permute-start.4 = (bf16[1,64,2048]{2,1,0:T(8,128)(2,1)S(1)}, bf16[1,64,2048]{2,1,0:T(8,128)(2,1)S(1)}, u32[]{:S(2)}, u32[]{:S(2)}) collective-permute-start(bf16[1,64,2048]{2,1,0:T(8,128)(2,1)S(1)} %get-tuple-element.24), channel_id=1, source_target_pairs={{0,4},{4,0},{8,12},{12,8},{16,20},{20,16},{24,28},{28,24},{1,5},{5... | collective-permute-start | bytes 786440 | tf_op jit(solution)/shard_map/ppermute | solution.py:9
  33.1 19.6 %collective-permute-start.23 = (bf16[1,64,2048]{2,1,0:T(8,128)(2,1)S(1)}, bf16[1,64,2048]{2,1,0:T(8,128)(2,1)S(1)}, u32[]{:S(2)}, u32[]{:S(2)}) collective-permute-start(bf16[1,64,2048]{2,1,0:T(8,128)(2,1)S(1)} %get-tuple-element.20), channel_id=1, source_target_pairs={{0,28},{4,24},{8,20},{12,16},{16,12},{20,8},{24,4},{28,0},{1,29},{... | collective-permute-start | bytes 786440 | tf_op jit(solution)/shard_map/ppermute | solution.py:9
  37.2 20.8 %collective-permute-start.22 = (bf16[1,64,2048]{2,1,0:T(8,128)(2,1)S(1)}, bf16[1,64,2048]{2,1,0:T(8,128)(2,1)S(1)}, u32[]{:S(2)}, u32[]{:S(2)}) collective-permute-start(bf16[1,64,2048]{2,1,0:T(8,128)(2,1)S(1)} %get-tuple-element.19), channel_id=1, source_target_pairs={{0,24},{4,28},{8,16},{12,20},{16,8},{20,12},{24,0},{28,4},{1,25},{... | collective-permute-start | bytes 786440 | tf_op jit(solution)/shard_map/ppermute | solution.py:9
  43.8 15.7 %collective-permute-start.14 = (bf16[128,2048]{1,0:T(8,128)(2,1)S(1)}, bf16[128,2048]{1,0:T(8,128)(2,1)S(1)}, u32[]{:S(2)}, u32[]{:S(2)}) collective-permute-start(bf16[128,2048]{1,0:T(8,128)(2,1)S(1)} %bitcast.147), channel_id=1, source_target_pairs={{0,2},{1,3},{2,0},{3,1},{4,6},{5,7},{6,4},{7,5},{8,10},{9,11},{10,... | collective-permute-start | bytes 1572872 | tf_op jit(solution)/shard_map/ppermute | solution.py:9
  45.4 34.4 %collective-permute-start.33 = (bf16[1,64,2048]{2,1,0:T(8,128)(2,1)S(1)}, bf16[1,64,2048]{2,1,0:T(8,128)(2,1)S(1)}, u32[]{:S(2)}, u32[]{:S(2)}) collective-permute-start(bf16[1,64,2048]{2,1,0:T(8,128)(2,1)S(1)} %get-tuple-element.16), channel_id=1, source_target_pairs={{0,20},{4,16},{8,28},{12,24},{16,4},{20,0},{24,12},{28,8},{1,21},{... | collective-permute-start | bytes 786440 | tf_op jit(solution)/shard_map/ppermute | solution.py:9
  49.3 34.0 %collective-permute-start.32 = (bf16[1,64,2048]{2,1,0:T(8,128)(2,1)S(1)}, bf16[1,64,2048]{2,1,0:T(8,128)(2,1)S(1)}, u32[]{:S(2)}, u32[]{:S(2)}) collective-permute-start(bf16[1,64,2048]{2,1,0:T(8,128)(2,1)S(1)} %get-tuple-element.15), channel_id=1, source_target_pairs={{0,16},{4,20},{8,24},{12,28},{16,0},{20,4},{24,8},{28,12},{1,17},{... | collective-permute-start | bytes 786440 | tf_op jit(solution)/shard_map/ppermute | solution.py:9
  52.8 30.6 %collective-permute-start.16 = (bf16[128,2048]{1,0:T(8,128)(2,1)S(1)}, bf16[128,2048]{1,0:T(8,128)(2,1)S(1)}, u32[]{:S(2)}, u32[]{:S(2)}) collective-permute-start(bf16[128,2048]{1,0:T(8,128)(2,1)S(1)} %bitcast.148), channel_id=1, source_target_pairs={{0,1},{1,0},{2,3},{3,2},{4,5},{5,4},{6,7},{7,6},{8,9},{9,8},{10,11... | collective-permute-start | bytes 1572872 | tf_op jit(solution)/shard_map/ppermute | solution.py:9
  58.0 26.9 %collective-permute-start.5 = (bf16[128,2048]{1,0:T(8,128)(2,1)S(1)}, bf16[128,2048]{1,0:T(8,128)(2,1)S(1)}, u32[]{:S(2)}, u32[]{:S(2)}) collective-permute-start(bf16[128,2048]{1,0:T(8,128)(2,1)S(1)} %bitcast.139), channel_id=1, source_target_pairs={{0,2},{1,3},{2,0},{3,1},{4,6},{5,7},{6,4},{7,5},{8,10},{9,11},{10,... | collective-permute-start | bytes 1572872 | tf_op jit(solution)/shard_map/ppermute | solution.py:9
  59.5 26.0 %collective-permute-start.15 = (bf16[128,2048]{1,0:T(8,128)(2,1)S(1)}, bf16[128,2048]{1,0:T(8,128)(2,1)S(1)}, u32[]{:S(2)}, u32[]{:S(2)}) collective-permute-start(bf16[128,2048]{1,0:T(8,128)(2,1)S(1)} %collective-permute-done.14), channel_id=1, source_target_pairs={{0,1},{1,0},{2,3},{3,2},{4,5},{5,4},{6,7},{7,6},{8,9},{9,8},{10,11... | collective-permute-start | bytes 1572872 | tf_op jit(solution)/shard_map/ppermute | solution.py:9
  83.3 30.2 %collective-permute-start.26 = (bf16[128,2048]{1,0:T(8,128)(2,1)S(1)}, bf16[128,2048]{1,0:T(8,128)(2,1)S(1)}, u32[]{:S(2)}, u32[]{:S(2)}) collective-permute-start(bf16[128,2048]{1,0:T(8,128)(2,1)S(1)} %bitcast.143), channel_id=1, source_target_pairs={{0,1},{1,0},{2,3},{3,2},{4,5},{5,4},{6,7},{7,6},{8,9},{9,8},{10,11... | collective-permute-start | bytes 1572872 | tf_op jit(solution)/shard_map/ppermute | solution.py:9
  83.4 14.9 %collective-permute-start.24 = (bf16[128,2048]{1,0:T(8,128)(2,1)S(1)}, bf16[128,2048]{1,0:T(8,128)(2,1)S(1)}, u32[]{:S(2)}, u32[]{:S(2)}) collective-permute-start(bf16[128,2048]{1,0:T(8,128)(2,1)S(1)} %bitcast.144), channel_id=1, source_target_pairs={{0,2},{1,3},{2,0},{3,1},{4,6},{5,7},{6,4},{7,5},{8,10},{9,11},{10,... | collective-permute-start | bytes 1572872 | tf_op jit(solution)/shard_map/ppermute | solution.py:9
  85.0 24.1 %collective-permute-start.34 = (bf16[128,2048]{1,0:T(8,128)(2,1)S(1)}, bf16[128,2048]{1,0:T(8,128)(2,1)S(1)}, u32[]{:S(2)}, u32[]{:S(2)}) collective-permute-start(bf16[128,2048]{1,0:T(8,128)(2,1)S(1)} %bitcast.135), channel_id=1, source_target_pairs={{0,2},{1,3},{2,0},{3,1},{4,6},{5,7},{6,4},{7,5},{8,10},{9,11},{10,... | collective-permute-start | bytes 1572872 | tf_op jit(solution)/shard_map/ppermute | solution.py:9
  85.5 23.5 %collective-permute-start.6 = (bf16[128,2048]{1,0:T(8,128)(2,1)S(1)}, bf16[128,2048]{1,0:T(8,128)(2,1)S(1)}, u32[]{:S(2)}, u32[]{:S(2)}) collective-permute-start(bf16[128,2048]{1,0:T(8,128)(2,1)S(1)} %collective-permute-done.5), channel_id=1, source_target_pairs={{0,1},{1,0},{2,3},{3,2},{4,5},{5,4},{6,7},{7,6},{8,9},{9,8},{10,11... | collective-permute-start | bytes 1572872 | tf_op jit(solution)/shard_map/ppermute | solution.py:9
  89.5 28.7 %collective-permute-start.36 = (bf16[128,2048]{1,0:T(8,128)(2,1)S(1)}, bf16[128,2048]{1,0:T(8,128)(2,1)S(1)}, u32[]{:S(2)}, u32[]{:S(2)}) collective-permute-start(bf16[128,2048]{1,0:T(8,128)(2,1)S(1)} %bitcast.136), channel_id=1, source_target_pairs={{0,1},{1,0},{2,3},{3,2},{4,5},{5,4},{6,7},{7,6},{8,9},{9,8},{10,11... | collective-permute-start | bytes 1572872 | tf_op jit(solution)/shard_map/ppermute | solution.py:9
  98.3 15.3 %collective-permute-start.25 = (bf16[128,2048]{1,0:T(8,128)(2,1)S(1)}, bf16[128,2048]{1,0:T(8,128)(2,1)S(1)}, u32[]{:S(2)}, u32[]{:S(2)}) collective-permute-start(bf16[128,2048]{1,0:T(8,128)(2,1)S(1)} %collective-permute-done.24), channel_id=1, source_target_pairs={{0,1},{1,0},{2,3},{3,2},{4,5},{5,4},{6,7},{7,6},{8,9},{9,8},{10,11... | collective-permute-start | bytes 1572872 | tf_op jit(solution)/shard_map/ppermute | solution.py:9
  109.0 13.7 %collective-permute-start.18 = (bf16[128,2048]{1,0:T(8,128)(2,1)S(1)}, bf16[128,2048]{1,0:T(8,128)(2,1)S(1)}, u32[]{:S(2)}, u32[]{:S(2)}) collective-permute-start(bf16[128,2048]{1,0:T(8,128)(2,1)S(1)} %get-tuple-element.12), channel_id=1, source_target_pairs={{0,1},{1,0},{2,3},{3,2},{4,5},{5,4},{6,7},{7,6},{8,9},{9,8},{10,11... | collective-permute-start | bytes 1572872 | tf_op jit(solution)/shard_map/ppermute | solution.py:9
  113.5 12.3 %collective-permute-start.17 = (bf16[128,2048]{1,0:T(8,128)(2,1)S(1)}, bf16[128,2048]{1,0:T(8,128)(2,1)S(1)}, u32[]{:S(2)}, u32[]{:S(2)}) collective-permute-start(bf16[128,2048]{1,0:T(8,128)(2,1)S(1)} %get-tuple-element.11), channel_id=1, source_target_pairs={{0,1},{1,0},{2,3},{3,2},{4,5},{5,4},{6,7},{7,6},{8,9},{9,8},{10,11... | collective-permute-start | bytes 1572872 | tf_op jit(solution)/shard_map/ppermute | solution.py:9
  118.3 22.1 %collective-permute-start.8 = (bf16[128,2048]{1,0:T(8,128)(2,1)S(1)}, bf16[128,2048]{1,0:T(8,128)(2,1)S(1)}, u32[]{:S(2)}, u32[]{:S(2)}) collective-permute-start(bf16[128,2048]{1,0:T(8,128)(2,1)S(1)} %get-tuple-element.9), channel_id=1, source_target_pairs={{0,1},{1,0},{2,3},{3,2},{4,5},{5,4},{6,7},{7,6},{8,9},{9,8},{10,11... | collective-permute-start | bytes 1572872 | tf_op jit(solution)/shard_map/ppermute | solution.py:9
  122.8 27.3 %collective-permute-start.27 = (bf16[128,2048]{1,0:T(8,128)(2,1)S(1)}, bf16[128,2048]{1,0:T(8,128)(2,1)S(1)}, u32[]{:S(2)}, u32[]{:S(2)}) collective-permute-start(bf16[128,2048]{1,0:T(8,128)(2,1)S(1)} %get-tuple-element.7), channel_id=1, source_target_pairs={{0,1},{1,0},{2,3},{3,2},{4,5},{5,4},{6,7},{7,6},{8,9},{9,8},{10,11... | collective-permute-start | bytes 1572872 | tf_op jit(solution)/shard_map/ppermute | solution.py:9
  123.7 14.9 %collective-permute-start.19 = (bf16[128,2048]{1,0:T(8,128)(2,1)S(1)}, bf16[128,2048]{1,0:T(8,128)(2,1)S(1)}, u32[]{:S(2)}, u32[]{:S(2)}) collective-permute-start(bf16[128,2048]{1,0:T(8,128)(2,1)S(1)} %add_convert_fusion.5), channel_id=1, source_target_pairs={{0,2},{1,3},{2,0},{3,1},{4,6},{5,7},{6,4},{7,5},{8,10},{9,11},{10,... | collective-permute-start | bytes 1572872 | tf_op jit(solution)/shard_map/ppermute | solution.py:9
  125.5 36.7 %collective-permute-start.37 = (bf16[128,2048]{1,0:T(8,128)(2,1)S(1)}, bf16[128,2048]{1,0:T(8,128)(2,1)S(1)}, u32[]{:S(2)}, u32[]{:S(2)}) collective-permute-start(bf16[128,2048]{1,0:T(8,128)(2,1)S(1)} %get-tuple-element.5), channel_id=1, source_target_pairs={{0,1},{1,0},{2,3},{3,2},{4,5},{5,4},{6,7},{7,6},{8,9},{9,8},{10,11... | collective-permute-start | bytes 1572872 | tf_op jit(solution)/shard_map/ppermute | solution.py:9
  125.8 24.0 %collective-permute-start.10 = (bf16[128,2048]{1,0:T(8,128)(2,1)S(1)}, bf16[128,2048]{1,0:T(8,128)(2,1)S(1)}, u32[]{:S(2)}, u32[]{:S(2)}) collective-permute-start(bf16[128,2048]{1,0:T(8,128)(2,1)S(1)} %add_convert_fusion.7), channel_id=1, source_target_pairs={{0,2},{1,3},{2,0},{3,1},{4,6},{5,7},{6,4},{7,5},{8,10},{9,11},{10,... | collective-permute-start | bytes 1572872 | tf_op jit(solution)/shard_map/ppermute | solution.py:9
  138.6 22.5 %collective-permute-start.29 = (bf16[128,2048]{1,0:T(8,128)(2,1)S(1)}, bf16[128,2048]{1,0:T(8,128)(2,1)S(1)}, u32[]{:S(2)}, u32[]{:S(2)}) collective-permute-start(bf16[128,2048]{1,0:T(8,128)(2,1)S(1)} %add_convert_fusion.3), channel_id=1, source_target_pairs={{0,2},{1,3},{2,0},{3,1},{4,6},{5,7},{6,4},{7,5},{8,10},{9,11},{10,... | collective-permute-start | bytes 1572872 | tf_op jit(solution)/shard_map/ppermute | solution.py:9
  140.4 31.0 %collective-permute-start.39 = (bf16[128,2048]{1,0:T(8,128)(2,1)S(1)}, bf16[128,2048]{1,0:T(8,128)(2,1)S(1)}, u32[]{:S(2)}, u32[]{:S(2)}) collective-permute-start(bf16[128,2048]{1,0:T(8,128)(2,1)S(1)} %add_convert_fusion.1), channel_id=1, source_target_pairs={{0,2},{1,3},{2,0},{3,1},{4,6},{5,7},{6,4},{7,5},{8,10},{9,11},{10,... | collective-permute-start | bytes 1572872 | tf_op jit(solution)/shard_map/ppermute | solution.py:9
  149.8 24.3 %collective-permute-start.21 = (bf16[1,64,2048]{2,1,0:T(8,128)(2,1)S(1)}, bf16[1,64,2048]{2,1,0:T(8,128)(2,1)S(1)}, u32[]{:S(2)}, u32[]{:S(2)}) collective-permute-start(bf16[1,64,2048]{2,1,0:T(8,128)(2,1)S(1)} %get-tuple-element.26), channel_id=1, source_target_pairs={{0,12},{4,8},{8,4},{12,0},{16,28},{20,24},{24,20},{28,16},{1,13},{... | collective-permute-start | bytes 786440 | tf_op jit(solution)/shard_map/ppermute | solution.py:9
  150.1 24.1 %collective-permute-start.20 = (bf16[1,64,2048]{2,1,0:T(8,128)(2,1)S(1)}, bf16[1,64,2048]{2,1,0:T(8,128)(2,1)S(1)}, u32[]{:S(2)}, u32[]{:S(2)}) collective-permute-start(bf16[1,64,2048]{2,1,0:T(8,128)(2,1)S(1)} %get-tuple-element.25), channel_id=1, source_target_pairs={{0,8},{4,12},{8,0},{12,4},{16,24},{20,28},{24,16},{28,20},{1,9},{5... | collective-permute-start | bytes 786440 | tf_op jit(solution)/shard_map/ppermute | solution.py:9
  161.0 16.9 %collective-permute-start.11 = (bf16[1,64,2048]{2,1,0:T(8,128)(2,1)S(1)}, bf16[1,64,2048]{2,1,0:T(8,128)(2,1)S(1)}, u32[]{:S(2)}, u32[]{:S(2)}) collective-permute-start(bf16[1,64,2048]{2,1,0:T(8,128)(2,1)S(1)} %get-tuple-element.22), channel_id=1, source_target_pairs={{0,4},{4,0},{8,12},{12,8},{16,20},{20,16},{24,28},{28,24},{1,5},{5... | collective-permute-start | bytes 786440 | tf_op jit(solution)/shard_map/ppermute | solution.py:9
  162.2 17.1 %collective-permute-start.31 = (bf16[1,64,2048]{2,1,0:T(8,128)(2,1)S(1)}, bf16[1,64,2048]{2,1,0:T(8,128)(2,1)S(1)}, u32[]{:S(2)}, u32[]{:S(2)}) collective-permute-start(bf16[1,64,2048]{2,1,0:T(8,128)(2,1)S(1)} %get-tuple-element.18), channel_id=1, source_target_pairs={{0,28},{4,24},{8,20},{12,16},{16,12},{20,8},{24,4},{28,0},{1,29},{... | collective-permute-start | bytes 786440 | tf_op jit(solution)/shard_map/ppermute | solution.py:9
  174.2 29.8 %collective-permute-start.41 = (bf16[1,64,2048]{2,1,0:T(8,128)(2,1)S(1)}, bf16[1,64,2048]{2,1,0:T(8,128)(2,1)S(1)}, u32[]{:S(2)}, u32[]{:S(2)}) collective-permute-start(bf16[1,64,2048]{2,1,0:T(8,128)(2,1)S(1)} %get-tuple-element.14), channel_id=1, source_target_pairs={{0,20},{4,16},{8,28},{12,24},{16,4},{20,0},{24,12},{28,8},{1,21},{... | collective-permute-start | bytes 786440 | tf_op jit(solution)/shard_map/ppermute | solution.py:9
  174.3 33.4 %collective-permute-start.40 = (bf16[1,64,2048]{2,1,0:T(8,128)(2,1)S(1)}, bf16[1,64,2048]{2,1,0:T(8,128)(2,1)S(1)}, u32[]{:S(2)}, u32[]{:S(2)}) collective-permute-start(bf16[1,64,2048]{2,1,0:T(8,128)(2,1)S(1)} %get-tuple-element.13), channel_id=1, source_target_pairs={{0,16},{4,20},{8,24},{12,28},{16,0},{20,4},{24,8},{28,12},{1,17},{... | collective-permute-start | bytes 786440 | tf_op jit(solution)/shard_map/ppermute | solution.py:9
  (17 other events, 243.6 us)
